TPU v7x, 32 devices: a whole 2x2x4 slice. The times are simulated.
32 devices in a mesh: sp: 4 (over x, core), dp: 8 (over z, y).
Axes of the slice: x: 2, y: 2, z: 4, core: 2. Of those that a mesh axis runs over, the one named last changes fastest.
Arguments:
- tokens: bfloat16 [8, 1536, 2048], P('dp', 'sp'), may hold values from -6 to 6
- w_value: bfloat16 [2048, 1024], P('dp'), may hold values from -0.125 to 0.125
- w_gate: bfloat16 [2048, 1024], P('dp'), may hold values from -0.125 to 0.125
- conv_taps: bfloat16 [31, 1024], replicated, may hold values from -1 to 1
- norm_gain: bfloat16 [1024], replicated, may hold values from 0.099609375 to 1.8984375
- w_out: bfloat16 [1024, 2048], P(None, 'dp'), may hold values from -0.1875 to 0.1875
Outputs:
- mixed: bfloat16 [8, 1536, 2048], P('dp', 'sp')
All inputs are finite; a program needn't handle non-finite values.
Results may differ from a plain program's by a relative error of at most 0.013.
Values may be sent and summed in bfloat16 or wider, within the bound.
No kernel may reach another device: no remote copies, remote signals or barrier semaphores. Data moves between devices by JAX's collectives and lax.ppermute only.
A program may use at most 64 MiB of HBM per device.

v0:
```python
import jax
import jax.numpy as jnp
from jax import lax
from jax.sharding import PartitionSpec as P

EPSILON = 1e-06


def passed_along(x, axis, by):
    length = lax.axis_size(axis)
    pairs = [(i, i + by) for i in range(length) if 0 <= i + by < length]
    return lax.ppermute(x, axis, pairs)


def depthwise_conv(signal, local_taps, left_pad):
    kernel_form = jnp.transpose(local_taps)[:, None, :]
    result = lax.conv_general_dilated(
        signal[None],
        kernel_form,
        (1,),
        [(left_pad, 0)],
        dimension_numbers=("NCH", "OIH", "NCH"),
        feature_group_count=signal.shape[0],
        preferred_element_type=jnp.float32,
    )
    return result[0].astype(jnp.bfloat16)


def body(tokens, w_value, w_gate, conv_taps, norm_gain, w_out):
    seq_rows = tokens[0]
    tok_count = seq_rows.shape[0]
    kernel_len = conv_taps.shape[0]
    value_sum = jnp.einsum(
        "dc,td->ct",
        lax.all_gather(w_value, "dp", axis=0, tiled=True),
        seq_rows,
        preferred_element_type=jnp.float32,
    )
    gate_sum = jnp.einsum(
        "dc,td->ct",
        lax.all_gather(w_gate, "dp", axis=0, tiled=True),
        seq_rows,
        preferred_element_type=jnp.float32,
    )
    gated = (value_sum * jax.nn.sigmoid(gate_sum)).astype(jnp.bfloat16)
    last_rows = gated[:, tok_count - (kernel_len - 1) :]
    earlier = passed_along(last_rows, "sp", 1)
    extended = jnp.concatenate([earlier, gated], axis=1)
    conv_out = depthwise_conv(extended, conv_taps, 0)
    wide = conv_out.astype(jnp.float32)
    chan_mean = jnp.mean(wide, 0, keepdims=True)
    centred = wide - chan_mean
    chan_var = jnp.mean(centred * centred, 0, keepdims=True)
    normed = centred * lax.rsqrt(chan_var + EPSILON) * norm_gain.astype(jnp.float32)[:, None]
    activated = (normed * jax.nn.sigmoid(normed)).astype(jnp.bfloat16)
    projected = jnp.einsum(
        "ct,cd->td",
        activated,
        lax.all_gather(w_out, "dp", axis=1, tiled=True),
        preferred_element_type=jnp.float32,
    ).astype(jnp.bfloat16)
    return projected[None]


def solution(mesh):
    placed = (P("dp", "sp", None), P("dp", None), P("dp", None), P(), P(), P(None, "dp"))
    return jax.shard_map(
        body, mesh=mesh, in_specs=placed, out_specs=P("dp", "sp", None), check_vma=False
    )
```

profile of v0, /device:TPU:0, one launch (start us, length us, event | category | flops | bytes accessed | tf_op | source)
XLA Modules:
  0.0 246.4 jit_solution(6799378059922831921)
XLA Ops:
  6.5 0.0 copy-start
  6.5 0.0 all-gather.6.cloned.1.call-start
  6.5 0.7 all-gather.6.cloned.1.call-update
  7.3 0.0 all-gather.4.cloned.1.call-start
  7.3 0.7 all-gather.4.cloned.1.call-update
  8.0 0.0 all-gather.8.cloned.1.call-start
  8.1 0.7 all-gather.8.cloned.1.call-update
  8.7 76.3 %all-gather.6.cloned.1.call-done = bf16[2048,1024]{1,0:T(8,128)(2,1)} async-done(((bf16[256,1024]{1,0:T(8,128)(2,1)}), bf16[2048,1024]{1,0:T(8,128)(2,1)}) %all-gather.6.cloned.1.call-update) | async-done | bytes 4194320 | tf_op jit(solution)/shard_map/all_gather | solution.py:41
  85.0 0.0 copy-done
  85.0 4.0 %fusion.4 = f32[1024,384]{0,1:T(8,128)S(1)} fusion(bf16[2048,1024]{1,0:T(8,128)(2,1)} %all-gather.6.cloned.1.call-done, bf16[1,384,2048]{2,1,0:T(8,128)(2,1)S(1)} %copy-done), kind=kOutput, calls=%fused_computation.8 | convolution fusion | flops 1610612736 | bytes 7340032 | tf_op jit(solution)/shard_map/dc,td->ct/dot_general | solution.py:39
  89.0 0.0 copy-start.1
  89.0 69.5 %all-gather.4.cloned.1.call-done = bf16[2048,1024]{1,0:T(8,128)(2,1)} async-done(((bf16[256,1024]{1,0:T(8,128)(2,1)}), bf16[2048,1024]{1,0:T(8,128)(2,1)}) %all-gather.4.cloned.1.call-update) | async-done | bytes 4194320 | tf_op jit(solution)/shard_map/all_gather | solution.py:35
  158.5 4.1 %multiply_convert_fusion.1 = bf16[1024,384]{0,1:T(8,128)(2,1)S(1)} fusion(f32[1024,384]{0,1:T(8,128)S(1)} %fusion.4, bf16[2048,1024]{1,0:T(8,128)(2,1)} %all-gather.4.cloned.1.call-done, bf16[1,384,2048]{2,1,0:T(8,128)(2,1)S(1)} %copy-done), kind=kOutput, calls=%fused_computation.12 | convolution fusion | flops 1612578816 | bytes 8126464 | tf_op jit(solution)/shard_map/dc,td->ct/dot_general | solution.py:33
  162.6 1.3 collective-permute-start
  163.9 0.0 copy-done.1
  163.9 0.9 collective-permute-done
  164.8 0.2 maximum_bitcast_fusion
  165.0 0.1 pad
  165.0 0.2 reshape.17
  165.2 0.0 copy-start.2
  165.2 0.0 copy-start.3
  165.2 0.5 copy.12
  165.7 0.1 slice.7
  165.8 0.2 copy-done.2
  166.0 0.0 copy-done.3
  166.0 3.8 %fusion.17 = f32[8,52,1024]{2,0,1:T(8,128)S(1)} fusion(bf16[1024,1,7,30]{0,2,3,1:T(8,128)(2,1)S(1)} %slice.7, bf16[1024,1,8,52]{0,2,3,1:T(8,128)(2,1)S(1)} %copy.12, pred[8,52]{0,1:T(8,128)(4,1)S(1)} %copy-done.3, bf16[1024,1,31]{0,2,1:T(8,128)(2,1)S(1)} %bitcast.35), kind=kOutput, calls=%fused_computation.20 | convolution fusion | flops 31719424 | bytes 3049888 | tf_op jit(solution)/shard_map/conv_general_dilated | solution.py:17
  169.8 2.2 copy.14
  172.1 1.6 reshape.21
  173.7 0.2 slice_reduce_fusion
  173.8 0.3 multiply_reduce_fusion
  174.1 60.3 %all-gather.8.cloned.1.call-done = bf16[1024,2048]{1,0:T(8,128)(2,1)} async-done(((bf16[1024,256]{1,0:T(8,128)(2,1)}), bf16[1024,2048]{1,0:T(8,128)(2,1)}) %all-gather.8.cloned.1.call-update) | async-done | bytes 4194320 | tf_op jit(solution)/shard_map/all_gather | solution.py:59
  234.5 5.5 %fusion.1 = bf16[1,384,2048]{2,1,0:T(8,128)(2,1)} fusion(bf16[1024,2048]{1,0:T(8,128)(2,1)} %all-gather.8.cloned.1.call-done, f32[1,416,1024]{2,1,0:T(8,128)S(1)} %reshape.21, f32[1024]{0:T(1024)S(1)} %convert_element_type.26, f32[384]{0:T(512)S(1)} %add_rsqrt_fusion, f32[384]{0:T(512)S(1)} %broadcast_multiply_fusion), kind=kOutput, calls=%fused_computation.3 | convolution fusion | flops 1614544896 | bytes 7348224 | tf_op jit(solution)/shard_map/ct,cd->td/dot_general | solution.py:56
  (4 shorter events, 0.0 us)
Async XLA Ops:
  6.5 78.5 %copy-start = (bf16[1,384,2048]{2,1,0:T(8,128)(2,1)S(1)}, bf16[1,384,2048]{2,1,0:T(8,128)(2,1)}, u32[]{:S(2)}) copy-start(bf16[1,384,2048]{2,1,0:T(8,128)(2,1)} %param.6) | copy-start | bytes 4718596
  6.5 78.5 %all-gather.6.cloned.1.call-start = ((), (), s32[]{:S(2)}) async-start(), calls=%async_computation.1 | async-start | bytes 4718592 | tf_op jit(solution)/shard_map/all_gather | solution.py:41
  7.3 151.2 %all-gather.4.cloned.1.call-start = ((), (), s32[]{:S(2)}) async-start(), calls=%async_computation | async-start | bytes 4718592 | tf_op jit(solution)/shard_map/all_gather | solution.py:35
  8.0 226.4 %all-gather.8.cloned.1.call-start = ((), (), s32[]{:S(2)}) async-start(), calls=%async_computation.2 | async-start | bytes 4718592 | tf_op jit(solution)/shard_map/all_gather | solution.py:59
  89.0 74.9 %copy-start.1 = (bf16[1024]{0:T(1024)(128)(2,1)S(1)}, bf16[1024]{0:T(1024)(128)(2,1)}, u32[]{:S(2)}) copy-start(bf16[1024]{0:T(1024)(128)(2,1)} %param.10) | copy-start | bytes 6148
  162.6 2.2 collective-permute-start
  165.2 0.8 copy-start.2
  165.2 0.8 copy-start.3
Sparse Core Ops, SparseCore 0:
  9.5 75.5 all-gather.5
  87.1 71.3 all-gather.3
  160.5 73.8 all-gather.7
where the time goes:
time: 247 us; the launch traced here: 246 us
  waiting for transfers between devices  209 us (85%)
  matrix products  17.3 us (7%)
  between operations  13.2 us (5%)
  local copies, waits for them, and re-layouts  4.87 us (2%)
    all_gather x1, waiting for transfers between devices, body(): lax.all_gather(w_gate, 'dp', axis=0, tiled=True)  76.3 us
    all_gather x1, waiting for transfers between devices, body(): lax.all_gather(w_value, 'dp', axis=0, tiled=True)  69.5 us
    all_gather x1, waiting for transfers between devices, body(): lax.all_gather(w_out, 'dp', axis=1, tiled=True)  60.3 us
    dot_general x1, matrix products, body(): jnp.einsum('ct,cd->td', activated, lax.all_gather(w_out, 'dp', axis=1, ti...  5.46 us
  transfers between devices with their start and end apart: 4, of which 4 were waited for; matrix products, arithmetic and copies ran while one was open for 7% of the time, Pallas kernels for 0%

commit v1 on v0

--- a/solution.py
+++ b/solution.py
@@ -4,6 +4,22 @@
 from jax.sharding import PartitionSpec as P
 
 EPSILON = 1e-06
+
+
+def summed_both_ways(array, axis, dim, product):
+    size, position, rows = (lax.axis_size(axis), lax.axis_index(axis), array.shape[dim])
+    right = [(i, (i + 1) % size) for i in range(size)]
+    left = [(i, (i - 1) % size) for i in range(size)]
+    middle = size // 2
+    from_left = from_right = array
+    total = product(array, position * rows)
+    for step in range(1, middle + 1):
+        from_left = lax.ppermute(from_left, axis, right)
+        if step < size - middle:
+            from_right = lax.ppermute(from_right, axis, left)
+            total = total + product(from_right, (position + step) % size * rows)
+        total = total + product(from_left, (position - step) % size * rows)
+    return total
 
 
 def passed_along(x, axis, by):
@@ -36,11 +52,16 @@
         seq_rows,
         preferred_element_type=jnp.float32,
     )
-    gate_sum = jnp.einsum(
-        "dc,td->ct",
-        lax.all_gather(w_gate, "dp", axis=0, tiled=True),
-        seq_rows,
-        preferred_element_type=jnp.float32,
+    gate_sum = summed_both_ways(
+        w_gate,
+        "dp",
+        0,
+        lambda own_block, start: jnp.einsum(
+            "dc,td->ct",
+            own_block,
+            lax.dynamic_slice_in_dim(seq_rows, start, own_block.shape[0], axis=1),
+            preferred_element_type=jnp.float32,
+        ),
     )
     gated = (value_sum * jax.nn.sigmoid(gate_sum)).astype(jnp.bfloat16)
     last_rows = gated[:, tok_count - (kernel_len - 1) :]

time: 247 us -> 223 us (0.903)
  waiting for transfers between devices: 209 us -> 151 us
  starting transfers between devices: 1.37 us -> 21.6 us
  matrix products: 17.3 us -> 29.3 us
    all_gather x1 -> x0, waiting for transfers between devices: 76.3 us -> none  [body(): lax.all_gather(w_gate, 'dp', axis=0, tiled=True)]
    ppermute x0 -> x7, waiting for transfers between devices: none -> 72 us  [the longest x4 72 us: summed_both_ways(): from_left = lax.ppermute(from_left, axis, right)]
    all_gather x1, waiting for transfers between devices: 69.5 us -> 21.1 us  [body(): lax.all_gather(w_value, 'dp', axis=0, tiled=True)]
    ppermute x0 -> x7, starting transfers between devices: none -> 19.7 us  [the longest x4 10.5 us: summed_both_ways(): from_left = lax.ppermute(from_left, axis, right)]
    dot_general x1 -> x8, matrix products: 3.97 us -> 15.9 us  [body(): jnp.einsum('dc,td->ct', own_block, lax.dynamic_slice_in_dim(seq_rows, sta...]
    all_gather x1, waiting for transfers between devices: 60.3 us -> 56.2 us  [body(): lax.all_gather(w_out, 'dp', axis=1, tiled=True)]
  transfers between devices with their start and end apart: 4 -> 10, of which waited for: 4 -> 6; matrix products, arithmetic and copies ran while one was open for 7% -> 13% of each run, Pallas kernels for 0% -> 0%
where the time goes in v1:
time: 223 us; the launch traced here: 222 us
  waiting for transfers between devices  151 us (68%)
  matrix products  29.3 us (13%)
  starting transfers between devices  21.6 us (10%)
  between operations  13.6 us (6%)
  local copies, waits for them, and re-layouts  5.65 us (3%)
    ppermute x4, waiting for transfers between devices, summed_both_ways(): from_left = lax.ppermute(from_left, axis, right)  72 us
    all_gather x1, waiting for transfers between devices, body(): lax.all_gather(w_out, 'dp', axis=1, tiled=True)  56.2 us
    all_gather x1, waiting for transfers between devices, body(): lax.all_gather(w_value, 'dp', axis=0, tiled=True)  21.1 us
    dot_general x8, matrix products, body(): jnp.einsum('dc,td->ct', own_block, lax.dynamic_slice_in_dim(seq_rows, sta...  15.9 us
    ppermute x4, starting transfers between devices, summed_both_ways(): from_left = lax.ppermute(from_left, axis, right)  10.5 us
    ppermute x3, starting transfers between devices, summed_both_ways(): from_right = lax.ppermute(from_right, axis, left)  9.21 us
    dot_general x1, matrix products, body(): jnp.einsum('ct,cd->td', activated, lax.all_gather(w_out, 'dp', axis=1, ti...  5.46 us
  transfers between devices with their start and end apart: 10, of which 6 were waited for; matrix products, arithmetic and copies ran while one was open for 13% of the time, Pallas kernels for 0%

profile of v1, /device:TPU:0, one launch (start us, length us, event | category | flops | bytes accessed | tf_op | source)
XLA Modules:
  0.0 222.1 jit_solution(1190437085670845615)
XLA Ops:
  6.5 0.0 copy-start
  6.5 0.0 all-gather.3.cloned.1.call-start
  6.5 0.7 all-gather.3.cloned.1.call-update
  7.3 0.0 all-gather.5.cloned.1.call-start
  7.3 0.7 all-gather.5.cloned.1.call-update
  8.0 3.0 %collective-permute-start.1 = (bf16[256,1024]{1,0:T(8,128)(2,1)}, bf16[256,1024]{1,0:T(8,128)(2,1)}, u32[]{:S(2)}, u32[]{:S(2)}) collective-permute-start(bf16[256,1024]{1,0:T(8,128)(2,1)} %param.8), channel_id=1, source_target_pairs={{0,1},{1,2},{2,3},{3,4},{4,5},{5,6},{6,7},{7,0},{8,9},{9,10},{10,1... | collective-permute-start | bytes 1572872 | tf_op jit(solution)/shard_map/ppermute | solution.py:17
  11.1 3.1 %collective-permute-start = (bf16[256,1024]{1,0:T(8,128)(2,1)}, bf16[256,1024]{1,0:T(8,128)(2,1)}, u32[]{:S(2)}, u32[]{:S(2)}) collective-permute-start(bf16[256,1024]{1,0:T(8,128)(2,1)} %param.8), channel_id=1, source_target_pairs={{0,7},{1,0},{2,1},{3,2},{4,3},{5,4},{6,5},{7,6},{8,15},{9,8},{10,9... | collective-permute-start | bytes 1572872 | tf_op jit(solution)/shard_map/ppermute | solution.py:19
  14.2 0.0 copy-done
  14.2 1.4 fusion.35
  15.6 23.8 %collective-permute-done.1 = bf16[256,1024]{1,0:T(8,128)(2,1)} collective-permute-done((bf16[256,1024]{1,0:T(8,128)(2,1)}, bf16[256,1024]{1,0:T(8,128)(2,1)}, u32[]{:S(2)}, u32[]{:S(2)}) %collective-permute-start.1) | collective-permute-done | bytes 524320 | tf_op jit(solution)/shard_map/ppermute | solution.py:17
  39.4 2.5 %collective-permute-start.3 = (bf16[256,1024]{1,0:T(8,128)(2,1)}, bf16[256,1024]{1,0:T(8,128)(2,1)S(1)}, u32[]{:S(2)}, u32[]{:S(2)}) collective-permute-start(bf16[256,1024]{1,0:T(8,128)(2,1)} %collective-permute-done.1), channel_id=1, source_target_pairs={{0,1},{1,2},{2,3},{3,4},{4,5},{5,6},{6,7},{7,0},{8,9},{9,10},{10,1... | collective-permute-start | bytes 1572872 | tf_op jit(solution)/shard_map/ppermute | solution.py:17
  41.9 0.0 collective-permute-done
  41.9 3.0 %collective-permute-start.2 = (bf16[256,1024]{1,0:T(8,128)(2,1)}, bf16[256,1024]{1,0:T(8,128)(2,1)S(1)}, u32[]{:S(2)}, u32[]{:S(2)}) collective-permute-start(bf16[256,1024]{1,0:T(8,128)(2,1)} %collective-permute-done), channel_id=1, source_target_pairs={{0,7},{1,0},{2,1},{3,2},{4,3},{5,4},{6,5},{7,6},{8,15},{9,8},{10,9... | collective-permute-start | bytes 1572872 | tf_op jit(solution)/shard_map/ppermute | solution.py:19
  44.9 2.6 %fusion.31 = f32[384,1024]{1,0:T(8,128)} fusion(bf16[256,1024]{1,0:T(8,128)(2,1)} %collective-permute-done.1, bf16[1,384,2048]{2,1,0:T(8,128)(2,1)S(1)} %copy-done, s32[]{:T(128)S(6)} %select_n.59), kind=kOutput, calls=%fused_computation.35 | convolution fusion | flops 201326592 | bytes 2293764 | tf_op jit(solution)/shard_map/dc,td->ct/dot_general | solution.py:59
  47.6 2.6 %fusion.33 = f32[384,1024]{1,0:T(8,128)} fusion(bf16[256,1024]{1,0:T(8,128)(2,1)} %collective-permute-done, bf16[1,384,2048]{2,1,0:T(8,128)(2,1)S(1)} %copy-done, s32[]{:T(128)S(6)} %select_n.57), kind=kOutput, calls=%fused_computation.37 | convolution fusion | flops 201326592 | bytes 2293764 | tf_op jit(solution)/shard_map/dc,td->ct/dot_general | solution.py:59
  50.1 21.8 %collective-permute-done.3 = bf16[256,1024]{1,0:T(8,128)(2,1)S(1)} collective-permute-done((bf16[256,1024]{1,0:T(8,128)(2,1)}, bf16[256,1024]{1,0:T(8,128)(2,1)S(1)}, u32[]{:S(2)}, u32[]{:S(2)}) %collective-permute-start.3) | collective-permute-done | bytes 524320 | tf_op jit(solution)/shard_map/ppermute | solution.py:17
  71.9 2.4 %collective-permute-start.5 = (bf16[256,1024]{1,0:T(8,128)(2,1)S(1)}, bf16[256,1024]{1,0:T(8,128)(2,1)}, u32[]{:S(2)}, u32[]{:S(2)}) collective-permute-start(bf16[256,1024]{1,0:T(8,128)(2,1)S(1)} %collective-permute-done.3), channel_id=1, source_target_pairs={{0,1},{1,2},{2,3},{3,4},{4,5},{5,6},{6,7},{7,0},{8,9},{9,10},{10,1... | collective-permute-start | bytes 1572872 | tf_op jit(solution)/shard_map/ppermute | solution.py:17
  74.3 0.0 collective-permute-done.2
  74.3 3.1 %collective-permute-start.4 = (bf16[256,1024]{1,0:T(8,128)(2,1)S(1)}, bf16[256,1024]{1,0:T(8,128)(2,1)S(1)}, u32[]{:S(2)}, u32[]{:S(2)}) collective-permute-start(bf16[256,1024]{1,0:T(8,128)(2,1)S(1)} %collective-permute-done.2), channel_id=1, source_target_pairs={{0,7},{1,0},{2,1},{3,2},{4,3},{5,4},{6,5},{7,6},{8,15},{9,8},{10,9... | collective-permute-start | bytes 1572872 | tf_op jit(solution)/shard_map/ppermute | solution.py:19
  77.4 1.6 fusion.27
  79.0 1.5 fusion.29
  80.5 26.4 %collective-permute-done.5 = bf16[256,1024]{1,0:T(8,128)(2,1)} collective-permute-done((bf16[256,1024]{1,0:T(8,128)(2,1)S(1)}, bf16[256,1024]{1,0:T(8,128)(2,1)}, u32[]{:S(2)}, u32[]{:S(2)}) %collective-permute-start.5) | collective-permute-done | bytes 524320 | tf_op jit(solution)/shard_map/ppermute | solution.py:17
  106.9 2.6 %collective-permute-start.6 = (bf16[256,1024]{1,0:T(8,128)(2,1)}, bf16[256,1024]{1,0:T(8,128)(2,1)}, u32[]{:S(2)}, u32[]{:S(2)}) collective-permute-start(bf16[256,1024]{1,0:T(8,128)(2,1)} %collective-permute-done.5), channel_id=1, source_target_pairs={{0,1},{1,2},{2,3},{3,4},{4,5},{5,6},{6,7},{7,0},{8,9},{9,10},{10,1... | collective-permute-start | bytes 1572872 | tf_op jit(solution)/shard_map/ppermute | solution.py:17
  109.5 2.6 %fusion.23 = f32[384,1024]{1,0:T(8,128)} fusion(bf16[256,1024]{1,0:T(8,128)(2,1)} %collective-permute-done.5, bf16[1,384,2048]{2,1,0:T(8,128)(2,1)S(1)} %copy-done, s32[]{:T(128)S(6)} %select_n.67), kind=kOutput, calls=%fused_computation.27 | convolution fusion | flops 201326592 | bytes 2293764 | tf_op jit(solution)/shard_map/dc,td->ct/dot_general | solution.py:59
  112.1 0.0 collective-permute-done.4
  112.1 1.5 fusion.25
  113.7 21.1 %all-gather.3.cloned.1.call-done = bf16[2048,1024]{1,0:T(8,128)(2,1)} async-done(((bf16[256,1024]{1,0:T(8,128)(2,1)}), bf16[2048,1024]{1,0:T(8,128)(2,1)}) %all-gather.3.cloned.1.call-update) | async-done | bytes 4194320 | tf_op jit(solution)/shard_map/all_gather | solution.py:51
  134.7 0.0 copy-start.1
  134.7 0.0 copy-start.2
  134.7 0.0 copy-start.3
  134.7 0.0 copy-start.4
  134.7 0.0 copy-start.5
  134.7 0.0 copy-start.6
  134.7 4.1 %fusion.3 = f32[1024,384]{0,1:T(8,128)S(1)} fusion(bf16[2048,1024]{1,0:T(8,128)(2,1)} %all-gather.3.cloned.1.call-done, bf16[1,384,2048]{2,1,0:T(8,128)(2,1)S(1)} %copy-done), kind=kOutput, calls=%fused_computation.8 | convolution fusion | flops 1610612736 | bytes 7340032 | tf_op jit(solution)/shard_map/dc,td->ct/dot_general | solution.py:49
  138.9 0.0 copy-start.7
  138.9 0.0 collective-permute-done.6
  138.9 0.0 copy-done.1
  138.9 0.0 copy-done.2
  138.9 0.0 copy-done.3
  138.9 0.0 copy-done.4
  138.9 0.3 copy-done.5
  139.3 0.4 copy-done.6
  139.7 2.0 fusion.2
  141.7 1.8 collective-permute-start.7
  143.5 0.0 copy-done.7
  143.6 0.7 collective-permute-done.7
  144.2 0.2 maximum_bitcast_fusion
  144.5 0.1 pad
  144.5 0.2 reshape.25
  144.7 0.0 copy-start.8
  144.7 0.0 copy-start.9
  144.7 0.5 copy.11
  145.2 0.1 slice.7
  145.3 0.2 copy-done.8
  145.5 0.0 copy-done.9
  145.5 3.8 %fusion.14 = f32[8,52,1024]{2,0,1:T(8,128)S(1)} fusion(bf16[1024,1,7,30]{0,2,3,1:T(8,128)(2,1)S(1)} %slice.7, bf16[1024,1,8,52]{0,2,3,1:T(8,128)(2,1)S(1)} %copy.11, pred[8,52]{0,1:T(8,128)(4,1)S(1)} %copy-done.9, bf16[1024,1,31]{0,2,1:T(8,128)(2,1)S(1)} %bitcast.66), kind=kOutput, calls=%fused_computation.19 | convolution fusion | flops 31719424 | bytes 3049888 | tf_op jit(solution)/shard_map/conv_general_dilated | solution.py:33
  149.3 2.2 %copy.13 = f32[8,52,1024]{2,1,0:T(8,128)} copy(f32[8,52,1024]{2,0,1:T(8,128)S(1)} %fusion.14) | data formatting | bytes 3407872 | tf_op jit(solution)/shard_map/convert_element_type | solution.py:71
  151.6 1.6 reshape.29
  153.1 0.2 slice_reduce_fusion
  153.3 0.3 multiply_reduce_fusion
  153.6 56.2 %all-gather.5.cloned.1.call-done = bf16[1024,2048]{1,0:T(8,128)(2,1)} async-done(((bf16[1024,256]{1,0:T(8,128)(2,1)}), bf16[1024,2048]{1,0:T(8,128)(2,1)}) %all-gather.5.cloned.1.call-update) | async-done | bytes 4194320 | tf_op jit(solution)/shard_map/all_gather | solution.py:80
  209.8 5.5 %fusion.1 = bf16[1,384,2048]{2,1,0:T(8,128)(2,1)} fusion(bf16[1024,2048]{1,0:T(8,128)(2,1)} %all-gather.5.cloned.1.call-done, f32[1,416,1024]{2,1,0:T(8,128)S(1)} %reshape.29, f32[1024]{0:T(1024)S(1)} %convert_element_type.26, f32[384]{0:T(512)S(1)} %add_rsqrt_fusion, f32[384]{0:T(512)S(1)} %broadcast_multiply_fusion), kind=kOutput, calls=%fused_computation.3 | convolution fusion | flops 1614544896 | bytes 7348224 | tf_op jit(solution)/shard_map/ct,cd->td/dot_general | solution.py:77
  (4 shorter events, 0.0 us)
Async XLA Ops:
  6.5 7.6 %copy-start = (bf16[1,384,2048]{2,1,0:T(8,128)(2,1)S(1)}, bf16[1,384,2048]{2,1,0:T(8,128)(2,1)}, u32[]{:S(2)}) copy-start(bf16[1,384,2048]{2,1,0:T(8,128)(2,1)} %param.6) | copy-start | bytes 4718596
  6.5 128.2 %all-gather.3.cloned.1.call-start = ((), (), s32[]{:S(2)}) async-start(), calls=%async_computation | async-start | bytes 4718592 | tf_op jit(solution)/shard_map/all_gather | solution.py:51
  7.3 202.5 %all-gather.5.cloned.1.call-start = ((), (), s32[]{:S(2)}) async-start(), calls=%async_computation.1 | async-start | bytes 4718592 | tf_op jit(solution)/shard_map/all_gather | solution.py:80
  8.0 31.4 %collective-permute-start.1 = (bf16[256,1024]{1,0:T(8,128)(2,1)}, bf16[256,1024]{1,0:T(8,128)(2,1)}, u32[]{:S(2)}, u32[]{:S(2)}) collective-permute-start(bf16[256,1024]{1,0:T(8,128)(2,1)} %param.8), channel_id=1, source_target_pairs={{0,1},{1,2},{2,3},{3,4},{4,5},{5,6},{6,7},{7,0},{8,9},{9,10},{10,1... | collective-permute-start | bytes 1572872 | tf_op jit(solution)/shard_map/ppermute | solution.py:17
  11.1 30.8 %collective-permute-start = (bf16[256,1024]{1,0:T(8,128)(2,1)}, bf16[256,1024]{1,0:T(8,128)(2,1)}, u32[]{:S(2)}, u32[]{:S(2)}) collective-permute-start(bf16[256,1024]{1,0:T(8,128)(2,1)} %param.8), channel_id=1, source_target_pairs={{0,7},{1,0},{2,1},{3,2},{4,3},{5,4},{6,5},{7,6},{8,15},{9,8},{10,9... | collective-permute-start | bytes 1572872 | tf_op jit(solution)/shard_map/ppermute | solution.py:19
  39.4 32.5 %collective-permute-start.3 = (bf16[256,1024]{1,0:T(8,128)(2,1)}, bf16[256,1024]{1,0:T(8,128)(2,1)S(1)}, u32[]{:S(2)}, u32[]{:S(2)}) collective-permute-start(bf16[256,1024]{1,0:T(8,128)(2,1)} %collective-permute-done.1), channel_id=1, source_target_pairs={{0,1},{1,2},{2,3},{3,4},{4,5},{5,6},{6,7},{7,0},{8,9},{9,10},{10,1... | collective-permute-start | bytes 1572872 | tf_op jit(solution)/shard_map/ppermute | solution.py:17
  41.9 32.4 %collective-permute-start.2 = (bf16[256,1024]{1,0:T(8,128)(2,1)}, bf16[256,1024]{1,0:T(8,128)(2,1)S(1)}, u32[]{:S(2)}, u32[]{:S(2)}) collective-permute-start(bf16[256,1024]{1,0:T(8,128)(2,1)} %collective-permute-done), channel_id=1, source_target_pairs={{0,7},{1,0},{2,1},{3,2},{4,3},{5,4},{6,5},{7,6},{8,15},{9,8},{10,9... | collective-permute-start | bytes 1572872 | tf_op jit(solution)/shard_map/ppermute | solution.py:19
  71.9 35.0 %collective-permute-start.5 = (bf16[256,1024]{1,0:T(8,128)(2,1)S(1)}, bf16[256,1024]{1,0:T(8,128)(2,1)}, u32[]{:S(2)}, u32[]{:S(2)}) collective-permute-start(bf16[256,1024]{1,0:T(8,128)(2,1)S(1)} %collective-permute-done.3), channel_id=1, source_target_pairs={{0,1},{1,2},{2,3},{3,4},{4,5},{5,6},{6,7},{7,0},{8,9},{9,10},{10,1... | collective-permute-start | bytes 1572872 | tf_op jit(solution)/shard_map/ppermute | solution.py:17
  74.3 37.8 %collective-permute-start.4 = (bf16[256,1024]{1,0:T(8,128)(2,1)S(1)}, bf16[256,1024]{1,0:T(8,128)(2,1)S(1)}, u32[]{:S(2)}, u32[]{:S(2)}) collective-permute-start(bf16[256,1024]{1,0:T(8,128)(2,1)S(1)} %collective-permute-done.2), channel_id=1, source_target_pairs={{0,7},{1,0},{2,1},{3,2},{4,3},{5,4},{6,5},{7,6},{8,15},{9,8},{10,9... | collective-permute-start | bytes 1572872 | tf_op jit(solution)/shard_map/ppermute | solution.py:19
  106.9 31.9 %collective-permute-start.6 = (bf16[256,1024]{1,0:T(8,128)(2,1)}, bf16[256,1024]{1,0:T(8,128)(2,1)}, u32[]{:S(2)}, u32[]{:S(2)}) collective-permute-start(bf16[256,1024]{1,0:T(8,128)(2,1)} %collective-permute-done.5), channel_id=1, source_target_pairs={{0,1},{1,2},{2,3},{3,4},{4,5},{5,6},{6,7},{7,0},{8,9},{9,10},{10,1... | collective-permute-start | bytes 1572872 | tf_op jit(solution)/shard_map/ppermute | solution.py:17
  134.7 4.2 %copy-start.1 = (f32[384,1024]{1,0:T(8,128)S(1)}, f32[384,1024]{1,0:T(8,128)}, u32[]{:S(2)}) copy-start(f32[384,1024]{1,0:T(8,128)} %fusion.31) | copy-start | bytes 4718596
  134.7 4.2 %copy-start.2 = (f32[384,1024]{1,0:T(8,128)S(1)}, f32[384,1024]{1,0:T(8,128)}, u32[]{:S(2)}) copy-start(f32[384,1024]{1,0:T(8,128)} %fusion.33) | copy-start | bytes 4718596
  134.7 4.2 %copy-start.3 = (f32[384,1024]{1,0:T(8,128)S(1)}, f32[384,1024]{1,0:T(8,128)}, u32[]{:S(2)}) copy-start(f32[384,1024]{1,0:T(8,128)} %fusion.27) | copy-start | bytes 4718596
  134.7 4.2 %copy-start.4 = (f32[384,1024]{1,0:T(8,128)S(1)}, f32[384,1024]{1,0:T(8,128)}, u32[]{:S(2)}) copy-start(f32[384,1024]{1,0:T(8,128)} %fusion.29) | copy-start | bytes 4718596
  134.7 4.5 %copy-start.5 = (f32[384,1024]{1,0:T(8,128)S(1)}, f32[384,1024]{1,0:T(8,128)}, u32[]{:S(2)}) copy-start(f32[384,1024]{1,0:T(8,128)} %fusion.23) | copy-start | bytes 4718596
  134.7 5.0 %copy-start.6 = (f32[384,1024]{1,0:T(8,128)S(1)}, f32[384,1024]{1,0:T(8,128)}, u32[]{:S(2)}) copy-start(f32[384,1024]{1,0:T(8,128)} %fusion.25) | copy-start | bytes 4718596
  138.9 4.7 %copy-start.7 = (bf16[1024]{0:T(1024)(128)(2,1)S(1)}, bf16[1024]{0:T(1024)(128)(2,1)}, u32[]{:S(2)}) copy-start(bf16[1024]{0:T(1024)(128)(2,1)} %param.10) | copy-start | bytes 6148
  141.7 2.5 %collective-permute-start.7 = (bf16[1024,30]{0,1:T(8,128)(2,1)S(1)}, bf16[1024,30]{0,1:T(8,128)(2,1)S(1)}, u32[]{:S(2)}, u32[]{:S(2)}) collective-permute-start(bf16[1024,30]{0,1:T(8,128)(2,1)S(1)} %slice.6), channel_id=1, source_target_pairs={{0,8},{8,16},{16,24},{1,9},{9,17},{17,25},{2,10},{10,18},{18,26},{... | collective-permute-start | bytes 184328 | tf_op jit(solution)/shard_map/ppermute | solution.py:28
  144.7 0.8 copy-start.8
  144.7 0.8 copy-start.9
Sparse Core Ops, SparseCore 0:
  9.5 125.2 all-gather.2
  136.8 72.9 all-gather.4
